TPU v7x, 128 devices: a whole 4x4x4 slice. The times are simulated.
128 devices in a mesh: sp: 32 (over y, x, core), tp: 4 (over z).
Axes of the slice: x: 4, y: 4, z: 4, core: 2. Of those that a mesh axis runs over, the one named last changes fastest.
Arguments:
- sequence: bfloat16 [4, 1024, 1024], P(None, 'sp', 'tp'), may hold values from -6 to 6
- norm_gain: float32 [3, 1024], replicated, may hold values from 0.1 to 1.9
- weight_value: bfloat16 [3, 1024, 512], P(None, 'sp', 'tp'), may hold values from -0.1875 to 0.1875
- weight_outer: bfloat16 [3, 1024, 512], P(None, 'sp', 'tp'), may hold values from -0.1875 to 0.1875
- weight_inner: bfloat16 [3, 1024, 512], P(None, 'sp', 'tp'), may hold values from -0.1875 to 0.1875
- conv_taps: float32 [3, 3, 512], P(None, None, 'tp'), may hold values from -3 to 3
- weight_out: bfloat16 [3, 512, 1024], P(None, 'tp', 'sp'), may hold values from -0.25 to 0.25
Outputs:
- mixed: bfloat16 [4, 1024, 1024], P(None, 'sp', 'tp')
All inputs are finite; a program needn't handle non-finite values.
Results may differ from a plain program's by a relative error of at most 0.03.
Values may be sent and summed in bfloat16 or wider, within the bound.
A program may use at most 64 MiB of HBM per device.

v0:
```python
import jax
import jax.numpy as jnp
from jax import lax
from jax.sharding import PartitionSpec as P

LAYERS = 3


def folded(array, axis, dim, update, carry):
    whole = jax.tree.map(lambda part: lax.all_gather(part, axis, axis=dim, tiled=True), array)
    return update(carry, whole, jnp.int32(0))


def from_behind(value, axis, steps):
    count = lax.axis_size(axis)
    first, last = (max(0, -steps), min(count, count - steps))
    return lax.ppermute(value, axis, [(source, source + steps) for source in range(first, last)])


def over_all(slab, axis, dim, apply):
    everything = lax.all_gather(slab, axis, axis=dim, tiled=True)
    return apply(everything, jnp.int32(0))


def rms_rows(values, gain_row):
    wide = values.astype(jnp.float32)
    scaled = wide * lax.rsqrt(jnp.mean(wide * wide, axis=-1, keepdims=True) + 1e-06)
    return (scaled * gain_row).astype(jnp.bfloat16)


def body(sequence, norm_gain, weight_value, weight_outer, weight_inner, conv_taps, weight_out):
    current = sequence
    seq_count = sequence.shape[0]
    local_len = sequence.shape[1]
    channels = weight_value.shape[2]
    depth = conv_taps.shape[1]
    for layer_index in range(LAYERS):
        whole = lax.all_gather(current, "tp", axis=2, tiled=True)
        normed = rms_rows(whole, norm_gain[layer_index]).reshape(
            seq_count * local_len, whole.shape[2]
        )
        empty = jnp.zeros((normed.shape[0], channels), jnp.float32)

        def add_rows(running, weight_rows, offset):
            columns = lax.dynamic_slice_in_dim(normed, offset, weight_rows.shape[0], 1)
            return running + jnp.dot(columns, weight_rows, preferred_element_type=jnp.float32)

        sum_value = folded(weight_value[layer_index], "sp", 0, add_rows, empty)
        sum_outer = folded(weight_outer[layer_index], "sp", 0, add_rows, empty)
        sum_inner = folded(weight_inner[layer_index], "sp", 0, add_rows, empty)
        proj_value = sum_value.astype(jnp.bfloat16)
        proj_outer = sum_outer.astype(jnp.bfloat16)
        proj_inner = sum_inner.astype(jnp.bfloat16)
        product = (proj_inner.astype(jnp.float32) * proj_value.astype(jnp.float32)).reshape(
            seq_count, local_len, channels
        )
        last_rows = product[:, local_len - (depth - 1) :, :]
        before = from_behind(last_rows, "sp", 1)
        padded = jnp.concatenate([before, product], axis=1)
        filtered = conv_taps[layer_index, 0] * padded[:, 0:local_len]
        for offset in range(1, depth):
            filtered = (
                filtered + conv_taps[layer_index, offset] * padded[:, offset : offset + local_len]
            )
        gated = (
            proj_outer.astype(jnp.float32).reshape(seq_count, local_len, channels) * filtered
        ).astype(jnp.bfloat16)
        gated_rows = gated.reshape(seq_count * local_len, channels)

        def project_columns(weight_cols, offset):
            return jnp.dot(gated_rows, weight_cols, preferred_element_type=jnp.float32)

        terms = over_all(weight_out[layer_index], "sp", 1, project_columns)
        shares = lax.psum_scatter(
            terms.astype(jnp.bfloat16), "tp", scatter_dimension=1, tiled=True
        ).astype(jnp.float32)
        shares = shares.reshape(seq_count, local_len, shares.shape[1])
        current = (current.astype(jnp.float32) + shares).astype(jnp.bfloat16)
    return current


def solution(mesh):
    return jax.shard_map(
        body,
        mesh=mesh,
        in_specs=(
            P(None, "sp", "tp"),
            P(),
            P(None, "sp", "tp"),
            P(None, "sp", "tp"),
            P(None, "sp", "tp"),
            P(None, None, "tp"),
            P(None, "tp", "sp"),
        ),
        out_specs=P(None, "sp", "tp"),
        check_vma=False,
    )
```

profile of v0, /device:TPU:0, one launch (start us, length us, event | category | flops | bytes accessed | tf_op | source)
XLA Modules:
  0.0 380.7 jit_solution(10216382479463195660)
XLA Ops:
  6.5 0.8 fusion.58
  7.4 13.8 %all_gather.45 = bf16[4,32,1024]{2,1,0:T(8,128)(2,1)S(1)} all-gather(bf16[4,32,256]{2,1,0:T(8,128)(2,1)} %param.7), channel_id=1, replica_groups=mesh['sp'=32,'tp'=4] {'tp'}, dimensions={2}, use_global_device_ids=true | all-gather | bytes 327680 | tf_op jit(solution)/shard_map/all_gather | solution.py:38
  21.2 0.1 fusion.9
  21.3 0.6 copy-done.1
  21.9 25.3 %all-gather.1 = bf16[1,1024,128]{2,1,0:T(8,128)(2,1)S(1)} all-gather(bf16[1,32,128]{2,1,0:T(8,128)(2,1)S(1)} %get-tuple-element.15), channel_id=3, replica_groups=mesh['sp'=32,'tp'=4] {'sp'}, dimensions={1}, use_global_device_ids=true | all-gather | bytes 270336 | tf_op jit(solution)/shard_map/all_gather | solution.py:10
  47.2 24.2 %all-gather.2 = bf16[1,1024,128]{2,1,0:T(8,128)(2,1)S(1)} all-gather(bf16[1,32,128]{2,1,0:T(8,128)(2,1)S(1)} %get-tuple-element.12), channel_id=4, replica_groups=mesh['sp'=32,'tp'=4] {'sp'}, dimensions={1}, use_global_device_ids=true | all-gather | bytes 270336 | tf_op jit(solution)/shard_map/all_gather | solution.py:10
  71.4 0.1 fusion.11
  71.5 0.2 fusion.8
  71.8 0.2 fusion.7
  72.0 2.3 collective-permute-start
  74.3 22.6 %all-gather = bf16[1,1024,128]{2,1,0:T(8,128)(2,1)S(1)} all-gather(bf16[1,32,128]{2,1,0:T(8,128)(2,1)S(1)} %get-tuple-element.9), channel_id=2, replica_groups=mesh['sp'=32,'tp'=4] {'sp'}, dimensions={1}, use_global_device_ids=true | all-gather | bytes 270336 | tf_op jit(solution)/shard_map/all_gather | solution.py:10
  96.9 0.2 convolution_convert_fusion.11
  97.1 0.5 copy-done.5
  97.6 0.1 copy-done.4
  97.7 24.2 %all-gather.3 = bf16[1,128,1024]{1,2,0:T(8,128)(2,1)S(1)} all-gather(bf16[1,128,32]{1,2,0:T(8,128)(2,1)S(1)} %get-tuple-element.6), channel_id=5, replica_groups=mesh['sp'=32,'tp'=4] {'sp'}, dimensions={2}, use_global_device_ids=true | all-gather | bytes 270336 | tf_op jit(solution)/shard_map/all_gather | solution.py:21
  121.9 0.9 convolution_convert_fusion.2
  122.9 0.0 reduce-scatter.6.cloned.1.call-start
  122.9 22.6 %all-gather.5 = bf16[1,1024,128]{2,1,0:T(8,128)(2,1)S(1)} all-gather(bf16[1,32,128]{2,1,0:T(8,128)(2,1)S(1)} %get-tuple-element.16), channel_id=7, replica_groups=mesh['sp'=32,'tp'=4] {'sp'}, dimensions={1}, use_global_device_ids=true | all-gather | bytes 270336 | tf_op jit(solution)/shard_map/all_gather | solution.py:10
  145.6 24.2 %all-gather.6 = bf16[1,1024,128]{2,1,0:T(8,128)(2,1)S(1)} all-gather(bf16[1,32,128]{2,1,0:T(8,128)(2,1)S(1)} %get-tuple-element.13), channel_id=8, replica_groups=mesh['sp'=32,'tp'=4] {'sp'}, dimensions={1}, use_global_device_ids=true | all-gather | bytes 270336 | tf_op jit(solution)/shard_map/all_gather | solution.py:10
  169.8 22.8 %all-gather.4 = bf16[1,1024,128]{2,1,0:T(8,128)(2,1)S(1)} all-gather(bf16[1,32,128]{2,1,0:T(8,128)(2,1)S(1)} %get-tuple-element.10), channel_id=6, replica_groups=mesh['sp'=32,'tp'=4] {'sp'}, dimensions={1}, use_global_device_ids=true | all-gather | bytes 270336 | tf_op jit(solution)/shard_map/all_gather | solution.py:10
  192.5 24.3 %all-gather.7 = bf16[1,128,1024]{1,2,0:T(8,128)(2,1)S(1)} all-gather(bf16[1,128,32]{1,2,0:T(8,128)(2,1)S(1)} %get-tuple-element.7), channel_id=9, replica_groups=mesh['sp'=32,'tp'=4] {'sp'}, dimensions={2}, use_global_device_ids=true | all-gather | bytes 270336 | tf_op jit(solution)/shard_map/all_gather | solution.py:21
  216.9 0.9 fusion.32
  217.7 12.3 %all_gather.50 = bf16[4,32,1024]{2,1,0:T(8,128)(2,1)S(1)} all-gather(bf16[4,32,256]{2,1,0:T(8,128)(2,1)S(1)} %fusion.32), channel_id=1, replica_groups=mesh['sp'=32,'tp'=4] {'tp'}, dimensions={2}, use_global_device_ids=true | all-gather | bytes 327680 | tf_op jit(solution)/shard_map/all_gather | solution.py:38
  230.0 0.1 fusion.12
  230.1 0.1 fusion.14
  230.3 0.2 fusion.5
  230.5 0.2 fusion.4
  230.8 1.3 collective-permute-start.1
  232.0 0.2 convolution_convert_fusion.8
  232.3 0.6 collective-permute-done.1
  232.9 0.9 convolution_convert_fusion.1
  233.8 0.0 reduce-scatter.8.cloned.1.call-start
  233.9 27.6 %all-gather.9 = bf16[1,1024,128]{2,1,0:T(8,128)(2,1)S(1)} all-gather(bf16[1,32,128]{2,1,0:T(8,128)(2,1)S(1)} %get-tuple-element.14), channel_id=11, replica_groups=mesh['sp'=32,'tp'=4] {'sp'}, dimensions={1}, use_global_device_ids=true | all-gather | bytes 270336 | tf_op jit(solution)/shard_map/all_gather | solution.py:10
  261.5 23.0 %all-gather.10 = bf16[1,1024,128]{2,1,0:T(8,128)(2,1)S(1)} all-gather(bf16[1,32,128]{2,1,0:T(8,128)(2,1)S(1)} %get-tuple-element.11), channel_id=12, replica_groups=mesh['sp'=32,'tp'=4] {'sp'}, dimensions={1}, use_global_device_ids=true | all-gather | bytes 270336 | tf_op jit(solution)/shard_map/all_gather | solution.py:10
  284.4 23.8 %all-gather.8 = bf16[1,1024,128]{2,1,0:T(8,128)(2,1)S(1)} all-gather(bf16[1,32,128]{2,1,0:T(8,128)(2,1)S(1)} %get-tuple-element.8), channel_id=10, replica_groups=mesh['sp'=32,'tp'=4] {'sp'}, dimensions={1}, use_global_device_ids=true | all-gather | bytes 270336 | tf_op jit(solution)/shard_map/all_gather | solution.py:10
  308.3 23.0 %all-gather.11 = bf16[1,128,1024]{1,2,0:T(8,128)(2,1)S(1)} all-gather(bf16[1,128,32]{1,2,0:T(8,128)(2,1)S(1)} %get-tuple-element.5), channel_id=13, replica_groups=mesh['sp'=32,'tp'=4] {'sp'}, dimensions={2}, use_global_device_ids=true | all-gather | bytes 270336 | tf_op jit(solution)/shard_map/all_gather | solution.py:21
  331.2 0.9 fusion.31
  332.1 12.3 %all_gather.55 = bf16[4,32,1024]{2,1,0:T(8,128)(2,1)S(1)} all-gather(bf16[4,32,256]{2,1,0:T(8,128)(2,1)S(1)} %fusion.31), channel_id=1, replica_groups=mesh['sp'=32,'tp'=4] {'tp'}, dimensions={2}, use_global_device_ids=true | all-gather | bytes 327680 | tf_op jit(solution)/shard_map/all_gather | solution.py:38
  344.4 0.1 fusion.15
  344.5 0.1 fusion.17
  344.6 0.2 fusion.2
  344.9 0.2 fusion.1
  345.1 1.3 collective-permute-start.2
  346.4 0.2 convolution_convert_fusion.5
  346.6 0.6 collective-permute-done.2
  347.3 0.9 convolution_convert_fusion
  348.2 24.5 %reduce-scatter.8.cloned.1.call-done = bf16[128,256]{1,0:T(8,128)(2,1)} async-done(((bf16[128,1024]{1,0:T(8,128)(2,1)}), bf16[128,256]{1,0:T(8,128)(2,1)}) %reduce-scatter.8.cloned.1.call-update) | async-done | bytes 65552 | tf_op jit(solution)/shard_map/reduce_scatter | solution.py:74
  372.7 1.5 fusion.30
  (30 shorter events, 0.2 us)
Async XLA Ops:
  6.5 210.3 %reduce-scatter.4.cloned.1.call-start = ((), (), s32[]{:S(2)}) async-start(), calls=%async_computation.3 | async-start | bytes 327680 | tf_op jit(solution)/shard_map/reduce_scatter | solution.py:74
  21.2 0.7 copy-start.1
  21.9 25.3 %copy-start.2 = (bf16[3,32,128]{2,1,0:T(8,128)(2,1)S(1)}, bf16[3,32,128]{2,1,0:T(8,128)(2,1)}, u32[]{:S(2)}) copy-start(bf16[3,32,128]{2,1,0:T(8,128)(2,1)} %param.9) | copy-start | bytes 73732
  71.7 2.5 copy-start.3
  72.0 49.9 %collective-permute-start = (f32[4,2,128]{2,1,0:T(2,128)S(1)}, f32[4,2,128]{2,1,0:T(2,128)S(1)}, u32[]{:S(2)}, u32[]{:S(2)}) collective-permute-start(f32[4,2,128]{2,1,0:T(2,128)S(1)} %slice.132), channel_id=1, source_target_pairs={{0,4},{4,8},{8,12},{12,16},{16,20},{20,24},{24,28},{28,32},{32,36}... | collective-permute-start | bytes 12296 | tf_op jit(solution)/shard_map/ppermute | solution.py:17
  96.9 0.7 copy-start.5
  96.9 0.8 copy-start.4
  122.9 208.4 %reduce-scatter.6.cloned.1.call-start = ((), (), s32[]{:S(2)}) async-start(), calls=%async_computation.4 | async-start | bytes 327680 | tf_op jit(solution)/shard_map/reduce_scatter | solution.py:74
  192.5 24.3 %copy-start = (bf16[4,32,256]{2,1,0:T(8,128)(2,1)S(1)}, bf16[4,32,256]{2,1,0:T(8,128)(2,1)}, u32[]{:S(2)}) copy-start(bf16[4,32,256]{2,1,0:T(8,128)(2,1)} %param.7) | copy-start | bytes 196612
  230.8 2.1 collective-permute-start.1
  233.8 138.8 %reduce-scatter.8.cloned.1.call-start = ((), (), s32[]{:S(2)}) async-start(), calls=%async_computation.5 | async-start | bytes 327680 | tf_op jit(solution)/shard_map/reduce_scatter | solution.py:74
  345.1 2.1 collective-permute-start.2
Sparse Core Ops, SparseCore 0:
  123.0 19.6 reduce-scatter.3
  234.0 23.3 reduce-scatter.5
  348.3 24.3 reduce-scatter.7
where the time goes:
time: 382 us; the launch traced here: 381 us
  blocking collectives  326 us (85%)
  waiting for transfers between devices  25.7 us (7%)
  between operations  13.3 us (3%)
  starting transfers between devices  4.92 us (1%)
  matrix products  4.77 us (1%)
  other arithmetic  4.11 us (1%)
    all_gather x9, blocking collectives, folded(): lax.all_gather(part, axis, axis=dim, tiled=True)  216 us
    all_gather x3, blocking collectives, over_all(): everything = lax.all_gather(slab, axis, axis=dim, tiled=True)  71.5 us
    all_gather x3, blocking collectives, body(): whole = lax.all_gather(current, 'tp', axis=2, tiled=True)  38.3 us
    reduce_scatter x3, waiting for transfers between devices, body(): lax.psum_scatter(terms.astype(jnp.bfloat16), 'tp', scatter_dimension=1, t...  24.5 us
  transfers between devices with their start and end apart: 6, of which 3 were waited for; matrix products, arithmetic and copies ran while one was open for 0% of the time, Pallas kernels for 0%

commit v1 on v0

--- a/solution.py
+++ b/solution.py
@@ -4,6 +4,11 @@
 from jax.sharding import PartitionSpec as P
 
 LAYERS = 3
+
+
+def gather_by_exchange(value, axis, dim):
+    copies = jnp.concatenate([value] * lax.axis_size(axis), axis=dim)
+    return lax.all_to_all(copies, axis, dim, dim, tiled=True)
 
 
 def folded(array, axis, dim, update, carry):
@@ -35,7 +40,7 @@
     channels = weight_value.shape[2]
     depth = conv_taps.shape[1]
     for layer_index in range(LAYERS):
-        whole = lax.all_gather(current, "tp", axis=2, tiled=True)
+        whole = gather_by_exchange(current, "tp", 2)
         normed = rms_rows(whole, norm_gain[layer_index]).reshape(
             seq_count * local_len, whole.shape[2]
         )

time: 382 us -> 414 us (1.084)
  waiting for transfers between devices: 25.7 us -> 70.3 us
  blocking collectives: 326 us -> 288 us
  starting transfers between devices: 4.92 us -> 19.2 us
  local copies, waits for them, and re-layouts: 2.01 us -> 11.1 us
    reduce_scatter x3, waiting for transfers between devices: 24.5 us -> 68.5 us  [body(): lax.psum_scatter(terms.astype(jnp.bfloat16), 'tp', scatter_dimension=1, t...]
    all_gather x3 -> x0, blocking collectives: 38.3 us -> none  [body(): whole = lax.all_gather(current, 'tp', axis=2, tiled=True)]
    all_to_all x0 -> x3, starting transfers between devices: none -> 12.4 us  [gather_by_exchange(): return lax.all_to_all(copies, axis, dim, dim, tiled=True)]
    unnamed x12 -> x20, local copies, waits for them, and re-layouts: 1.13 us -> 7.2 us
  transfers between devices with their start and end apart: 6 -> 9, of which waited for: 3 -> 6; matrix products, arithmetic and copies ran while one was open for 0% -> 0% of each run, Pallas kernels for 0% -> 0%
where the time goes in v1:
time: 414 us; the launch traced here: 412 us
  blocking collectives  288 us (70%)
  waiting for transfers between devices  70.3 us (17%)
  starting transfers between devices  19.2 us (5%)
  between operations  13.4 us (3%)
  local copies, waits for them, and re-layouts  11.1 us (3%)
  other arithmetic  5.17 us (1%)
  matrix products  4.76 us (1%)
    all_gather x9, blocking collectives, folded(): lax.all_gather(part, axis, axis=dim, tiled=True)  216 us
    all_gather x3, blocking collectives, over_all(): everything = lax.all_gather(slab, axis, axis=dim, tiled=True)  72.6 us
    reduce_scatter x3, waiting for transfers between devices, body(): lax.psum_scatter(terms.astype(jnp.bfloat16), 'tp', scatter_dimension=1, t...  68.5 us
    all_to_all x3, starting transfers between devices, gather_by_exchange(): return lax.all_to_all(copies, axis, dim, dim, tiled=True)  12.4 us
  transfers between devices with their start and end apart: 9, of which 6 were waited for; matrix products, arithmetic and copies ran while one was open for 0% of the time, Pallas kernels for 0%

profile of v1, /device:TPU:0, one launch (start us, length us, event | category | flops | bytes accessed | tf_op | source)
XLA Modules:
  0.0 412.4 jit_solution(10823604273945362923)
XLA Ops:
  6.5 1.0 pad_maximum_fusion
  7.6 0.7 copy.29
  8.3 1.7 reshape.135
  9.9 5.5 %all-to-all-start = ((bf16[4,2,16384]{2,1,0:T(2,128)(2,1)}), bf16[4,2,16384]{2,1,0:T(2,128)(2,1)S(1)}, u32[]{:S(2)}, u32[]{:S(2)}) async-start(bf16[4,2,16384]{2,1,0:T(2,128)(2,1)} %reshape.135), calls=%async_computation | async-start | bytes 524288 | tf_op jit(solution)/shard_map/all_to_all | solution.py:11
  15.5 0.7 copy-done.1
  16.2 25.3 %all-gather.1 = bf16[1,1024,128]{2,1,0:T(8,128)(2,1)S(1)} all-gather(bf16[1,32,128]{2,1,0:T(8,128)(2,1)S(1)} %get-tuple-element.15), channel_id=3, replica_groups=mesh['sp'=32,'tp'=4] {'sp'}, dimensions={1}, use_global_device_ids=true | all-gather | bytes 270336 | tf_op jit(solution)/shard_map/all_gather | solution.py:15
  41.5 24.2 %all-gather.2 = bf16[1,1024,128]{2,1,0:T(8,128)(2,1)S(1)} all-gather(bf16[1,32,128]{2,1,0:T(8,128)(2,1)S(1)} %get-tuple-element.12), channel_id=4, replica_groups=mesh['sp'=32,'tp'=4] {'sp'}, dimensions={1}, use_global_device_ids=true | all-gather | bytes 270336 | tf_op jit(solution)/shard_map/all_gather | solution.py:15
  65.7 22.6 %all-gather = bf16[1,1024,128]{2,1,0:T(8,128)(2,1)S(1)} all-gather(bf16[1,32,128]{2,1,0:T(8,128)(2,1)S(1)} %get-tuple-element.9), channel_id=2, replica_groups=mesh['sp'=32,'tp'=4] {'sp'}, dimensions={1}, use_global_device_ids=true | all-gather | bytes 270336 | tf_op jit(solution)/shard_map/all_gather | solution.py:15
  88.4 24.2 %all-gather.3 = bf16[1,128,1024]{1,2,0:T(8,128)(2,1)S(1)} all-gather(bf16[1,128,32]{1,2,0:T(8,128)(2,1)S(1)} %get-tuple-element.6), channel_id=5, replica_groups=mesh['sp'=32,'tp'=4] {'sp'}, dimensions={2}, use_global_device_ids=true | all-gather | bytes 270336 | tf_op jit(solution)/shard_map/all_gather | solution.py:26
  112.6 0.5 reshape.136
  113.1 0.6 copy.30
  114.2 0.2 fusion.7
  114.5 2.3 collective-permute-start
  116.8 0.2 convolution_convert_fusion.11
  117.0 0.6 collective-permute-done
  117.6 0.9 convolution_convert_fusion.2
  118.6 22.9 %reduce-scatter.4.cloned.1.call-done = bf16[128,256]{1,0:T(8,128)(2,1)} async-done(((bf16[128,1024]{1,0:T(8,128)(2,1)}), bf16[128,256]{1,0:T(8,128)(2,1)}) %reduce-scatter.4.cloned.1.call-update) | async-done | bytes 65552 | tf_op jit(solution)/shard_map/reduce_scatter | solution.py:79
  141.5 0.9 fusion.32
  142.4 0.7 copy.31
  143.1 1.7 reshape.137
  144.7 3.4 all-to-all-start.1
  148.2 25.0 %all-gather.5 = bf16[1,1024,128]{2,1,0:T(8,128)(2,1)S(1)} all-gather(bf16[1,32,128]{2,1,0:T(8,128)(2,1)S(1)} %get-tuple-element.16), channel_id=7, replica_groups=mesh['sp'=32,'tp'=4] {'sp'}, dimensions={1}, use_global_device_ids=true | all-gather | bytes 270336 | tf_op jit(solution)/shard_map/all_gather | solution.py:15
  173.2 24.2 %all-gather.6 = bf16[1,1024,128]{2,1,0:T(8,128)(2,1)S(1)} all-gather(bf16[1,32,128]{2,1,0:T(8,128)(2,1)S(1)} %get-tuple-element.13), channel_id=8, replica_groups=mesh['sp'=32,'tp'=4] {'sp'}, dimensions={1}, use_global_device_ids=true | all-gather | bytes 270336 | tf_op jit(solution)/shard_map/all_gather | solution.py:15
  197.4 22.6 %all-gather.4 = bf16[1,1024,128]{2,1,0:T(8,128)(2,1)S(1)} all-gather(bf16[1,32,128]{2,1,0:T(8,128)(2,1)S(1)} %get-tuple-element.10), channel_id=6, replica_groups=mesh['sp'=32,'tp'=4] {'sp'}, dimensions={1}, use_global_device_ids=true | all-gather | bytes 270336 | tf_op jit(solution)/shard_map/all_gather | solution.py:15
  220.0 24.2 %all-gather.7 = bf16[1,128,1024]{1,2,0:T(8,128)(2,1)S(1)} all-gather(bf16[1,128,32]{1,2,0:T(8,128)(2,1)S(1)} %get-tuple-element.7), channel_id=9, replica_groups=mesh['sp'=32,'tp'=4] {'sp'}, dimensions={2}, use_global_device_ids=true | all-gather | bytes 270336 | tf_op jit(solution)/shard_map/all_gather | solution.py:26
  244.2 0.5 reshape.138
  244.7 0.6 copy.32
  246.1 2.3 collective-permute-start.1
  248.5 0.6 collective-permute-done.1
  249.2 0.9 convolution_convert_fusion.1
  250.1 22.8 %reduce-scatter.6.cloned.1.call-done = bf16[128,256]{1,0:T(8,128)(2,1)} async-done(((bf16[128,1024]{1,0:T(8,128)(2,1)}), bf16[128,256]{1,0:T(8,128)(2,1)}) %reduce-scatter.6.cloned.1.call-update) | async-done | bytes 65552 | tf_op jit(solution)/shard_map/reduce_scatter | solution.py:79
  272.9 0.9 fusion.31
  273.8 0.7 copy.33
  274.5 1.7 reshape.139
  276.2 3.4 all-to-all-start.2
  279.6 24.8 %all-gather.9 = bf16[1,1024,128]{2,1,0:T(8,128)(2,1)S(1)} all-gather(bf16[1,32,128]{2,1,0:T(8,128)(2,1)S(1)} %get-tuple-element.14), channel_id=11, replica_groups=mesh['sp'=32,'tp'=4] {'sp'}, dimensions={1}, use_global_device_ids=true | all-gather | bytes 270336 | tf_op jit(solution)/shard_map/all_gather | solution.py:15
  304.5 24.4 %all-gather.10 = bf16[1,1024,128]{2,1,0:T(8,128)(2,1)S(1)} all-gather(bf16[1,32,128]{2,1,0:T(8,128)(2,1)S(1)} %get-tuple-element.11), channel_id=12, replica_groups=mesh['sp'=32,'tp'=4] {'sp'}, dimensions={1}, use_global_device_ids=true | all-gather | bytes 270336 | tf_op jit(solution)/shard_map/all_gather | solution.py:15
  328.9 22.6 %all-gather.8 = bf16[1,1024,128]{2,1,0:T(8,128)(2,1)S(1)} all-gather(bf16[1,32,128]{2,1,0:T(8,128)(2,1)S(1)} %get-tuple-element.8), channel_id=10, replica_groups=mesh['sp'=32,'tp'=4] {'sp'}, dimensions={1}, use_global_device_ids=true | all-gather | bytes 270336 | tf_op jit(solution)/shard_map/all_gather | solution.py:15
  351.5 24.2 %all-gather.11 = bf16[1,128,1024]{1,2,0:T(8,128)(2,1)S(1)} all-gather(bf16[1,128,32]{1,2,0:T(8,128)(2,1)S(1)} %get-tuple-element.5), channel_id=13, replica_groups=mesh['sp'=32,'tp'=4] {'sp'}, dimensions={2}, use_global_device_ids=true | all-gather | bytes 270336 | tf_op jit(solution)/shard_map/all_gather | solution.py:26
  375.7 0.5 reshape.140
  376.2 0.6 copy.34
  377.3 0.2 fusion.1
  377.6 2.3 collective-permute-start.2
  379.8 0.2 convolution_convert_fusion.5
  380.0 0.6 collective-permute-done.2
  380.7 0.9 convolution_convert_fusion
  381.6 22.8 %reduce-scatter.8.cloned.1.call-done = bf16[128,256]{1,0:T(8,128)(2,1)} async-done(((bf16[128,1024]{1,0:T(8,128)(2,1)}), bf16[128,256]{1,0:T(8,128)(2,1)}) %reduce-scatter.8.cloned.1.call-update) | async-done | bytes 65552 | tf_op jit(solution)/shard_map/reduce_scatter | solution.py:79
  404.4 1.5 fusion.30
  (50 shorter events, 2.3 us)
Async XLA Ops:
  9.9 5.6 %copy-start.5 = (f32[3,1024]{1,0:T(4,128)S(1)}, f32[3,1024]{1,0:T(4,128)}, u32[]{:S(2)}) copy-start(f32[3,1024]{1,0:T(4,128)} %param.8) | copy-start | bytes 36868
  9.9 102.7 %all-to-all-start = ((bf16[4,2,16384]{2,1,0:T(2,128)(2,1)}), bf16[4,2,16384]{2,1,0:T(2,128)(2,1)S(1)}, u32[]{:S(2)}, u32[]{:S(2)}) async-start(bf16[4,2,16384]{2,1,0:T(2,128)(2,1)} %reshape.135), calls=%async_computation | async-start | bytes 524288 | tf_op jit(solution)/shard_map/all_to_all | solution.py:11
  15.5 0.7 copy-start.1
  15.5 126.0 %reduce-scatter.4.cloned.1.call-start = ((), (), s32[]{:S(2)}) async-start(), calls=%async_computation.6 | async-start | bytes 327680 | tf_op jit(solution)/shard_map/reduce_scatter | solution.py:79
  16.2 25.3 %copy-start.2 = (bf16[3,32,128]{2,1,0:T(8,128)(2,1)S(1)}, bf16[3,32,128]{2,1,0:T(8,128)(2,1)}, u32[]{:S(2)}) copy-start(bf16[3,32,128]{2,1,0:T(8,128)(2,1)} %param.9) | copy-start | bytes 73732
  41.5 24.2 %copy-start.3 = (bf16[3,32,128]{2,1,0:T(8,128)(2,1)S(1)}, bf16[3,32,128]{2,1,0:T(8,128)(2,1)}, u32[]{:S(2)}) copy-start(bf16[3,32,128]{2,1,0:T(8,128)(2,1)} %param.10) | copy-start | bytes 73732
  65.7 22.6 %copy-start.4 = (bf16[3,128,32]{1,2,0:T(8,128)(2,1)S(1)}, bf16[3,128,32]{1,2,0:T(8,128)(2,1)}, u32[]{:S(2)}) copy-start(bf16[3,128,32]{1,2,0:T(8,128)(2,1)} %param.13) | copy-start | bytes 73732
  88.4 24.2 %copy-start.6 = (f32[3,3,128]{2,1,0:T(4,128)S(1)}, f32[3,3,128]{2,1,0:T(4,128)}, u32[]{:S(2)}) copy-start(f32[3,3,128]{2,1,0:T(4,128)} %param.12) | copy-start | bytes 13828
  114.5 3.1 collective-permute-start
  118.5 22.9 %copy-start = (bf16[4,32,256]{2,1,0:T(8,128)(2,1)S(1)}, bf16[4,32,256]{2,1,0:T(8,128)(2,1)}, u32[]{:S(2)}) copy-start(bf16[4,32,256]{2,1,0:T(8,128)(2,1)} %param.7) | copy-start | bytes 196612
  144.7 99.5 %all-to-all-start.1 = ((bf16[4,2,16384]{2,1,0:T(2,128)(2,1)}), bf16[4,2,16384]{2,1,0:T(2,128)(2,1)S(1)}, u32[]{:S(2)}, u32[]{:S(2)}) async-start(bf16[4,2,16384]{2,1,0:T(2,128)(2,1)} %reshape.137), calls=%async_computation.2 | async-start | bytes 524288 | tf_op jit(solution)/shard_map/all_to_all | solution.py:11
  148.1 124.8 %reduce-scatter.6.cloned.1.call-start = ((), (), s32[]{:S(2)}) async-start(), calls=%async_computation.7 | async-start | bytes 327680 | tf_op jit(solution)/shard_map/reduce_scatter | solution.py:79
  246.1 3.1 collective-permute-start.1
  276.2 99.5 %all-to-all-start.2 = ((bf16[4,2,16384]{2,1,0:T(2,128)(2,1)}), bf16[4,2,16384]{2,1,0:T(2,128)(2,1)S(1)}, u32[]{:S(2)}, u32[]{:S(2)}) async-start(bf16[4,2,16384]{2,1,0:T(2,128)(2,1)} %reshape.139), calls=%async_computation.4 | async-start | bytes 524288 | tf_op jit(solution)/shard_map/all_to_all | solution.py:11
  279.6 124.8 %reduce-scatter.8.cloned.1.call-start = ((), (), s32[]{:S(2)}) async-start(), calls=%async_computation.8 | async-start | bytes 327680 | tf_op jit(solution)/shard_map/reduce_scatter | solution.py:79
  377.6 3.1 collective-permute-start.2
Sparse Core Ops, SparseCore 0:
  118.7 22.7 reduce-scatter.3
  250.2 22.6 reduce-scatter.5
  381.7 22.6 reduce-scatter.7
